TPU v7x, 32 devices: a whole 2x2x4 slice. The times are simulated.
32 devices in a mesh: grp: 2 (over y), ep: 4 (over z), tp: 4 (over x, core).
Axes of the slice: x: 2, y: 2, z: 4, core: 2. Of those that a mesh axis runs over, the one named last changes fastest.
Arguments:
- tokens: bfloat16 [2048, 2048], P(('grp', 'ep')), parts along dimension 0, may hold values from -6 to 6
- in_gain: bfloat16 [2048], replicated, may hold values from 0.099609375 to 1.8984375
- expert_ids: int32 [2048, 2], P(('grp', 'ep')), parts along dimension 0, may hold values from 0 to 3, all different within a row; in each aligned block of 256 rows (0 to 255, 256 to 511, ...) at most 256 rows name the same one
- route_weights: float32 [2048, 2], P(('grp', 'ep')), parts along dimension 0, may hold values from 0.1 to 1
- gate_weight: bfloat16 [4, 2048, 2048], P('ep', None, 'tp'), may hold values from -0.375 to 0.375
- up_weight: bfloat16 [4, 2048, 2048], P('ep', None, 'tp'), may hold values from -0.375 to 0.375
- down_weight: bfloat16 [4, 2048, 2048], P('ep', 'tp')
- out_gain: bfloat16 [2048], P('tp'), may hold values from 0.099609375 to 1.8984375
Outputs:
- normed_out: bfloat16 [2048, 2048], P(('grp', 'ep'), 'tp'), parts along dimension 0
There are 2 independent parts, one for each index of `grp`. A program takes and returns all parts, laid end to end along the dimension named above; an argument that names none is the same for every part. Nothing has to cross between parts.
Inputs may be any that keep to these rules, and one draw needn't show every extreme that they name: `expert_ids`: each row names 2 different experts. Among the 256 rows of one index of ep, no expert is named more than 256 times, a bound that some block reaches.
All inputs are finite; a program needn't handle non-finite values.
Results may differ from a plain program's by a relative error of at most 0.015.
Values may be sent and summed in bfloat16 or wider, within the bound.
A program may use at most 64 MiB of HBM per device.

v0:
```python
import functools

import jax
import jax.numpy as jnp
from jax import lax
from jax.experimental import pallas as pl
from jax.experimental.pallas import tpu as pltpu
from jax.sharding import PartitionSpec as P

eps = 1e-05
f32 = jnp.float32
bf16 = jnp.bfloat16


def layer_kernel(
    tok, gain, ids, rw, wg, wu, wd, og, out,
    xbuf, wgb, wub, wdb, xn, part, drecv, esend, erecv, fin, ret, sq,
    load_sem, zs, zr, xs, xr, ps, pr, ds, dr, es, er, fs, fr, qs, qr,
):
    z, p = lax.axis_index("ep"), lax.axis_index("tp")
    n_ep, n_q, rows, fb = xbuf.shape
    half, c = p // 2, p % 2
    mate = half * 2 + 1 - c
    across = (1 - half) * 2 + c
    diagonal = (1 - half) * 2 + 1 - c
    hi = z // 2
    order = (z, 1 - z + hi * 4, 2 - hi, 3 - 3 * hi)

    def remote(src, dst, s, r, **where):
        return pltpu.make_async_remote_copy(
            src_ref=src, dst_ref=dst, send_sem=s, recv_sem=r,
            device_id=where, device_id_type=pl.DeviceIdType.MESH,
        )

    loads = [
        pltpu.make_async_copy(tok.at[:, pl.ds(q * fb, fb)], xbuf.at[z, q], load_sem.at[q])
        for q in range(n_q)
    ]
    weights = [
        pltpu.make_async_copy(wg.at[0], wgb, load_sem.at[n_q]),
        pltpu.make_async_copy(wu.at[0], wub, load_sem.at[n_q + 1]),
        pltpu.make_async_copy(wd.at[0], wdb, load_sem.at[n_q + 2]),
    ]
    for copy in loads + weights:
        copy.start()
    barrier = pltpu.get_barrier_semaphore()
    for peer in (mate, across, diagonal):
        pl.semaphore_signal(barrier, inc=1, device_id={"tp": peer}, device_id_type=pl.DeviceIdType.MESH)
    for b in order[1:]:
        pl.semaphore_signal(barrier, inc=1, device_id={"ep": b}, device_id_type=pl.DeviceIdType.MESH)
    pl.semaphore_wait(barrier, 6)
    for copy in loads:
        copy.wait()

    sends = []

    def push(copy):
        copy.start()
        sends.append(copy)

    for b in order[1:]:
        push(remote(xbuf.at[z, p], xbuf.at[z, p], zs.at[b], zr.at[z], ep=b))

    def arrived(ref, sem):
        pltpu.make_async_copy(ref, ref, sem).wait()

    def stage_a(b):
        arrived(xbuf.at[b, p], zr.at[b])
        push(remote(xbuf.at[b, p], xbuf.at[b, p], xs.at[b], xr.at[b], tp=across))
        push(remote(xbuf.at[b, p], xbuf.at[b, p], ps.at[0, b], pr.at[0, b], tp=mate))

    def stage_b(b):
        arrived(xbuf.at[b, across], xr.at[b])
        push(remote(xbuf.at[b, across], xbuf.at[b, across], ps.at[1, b], pr.at[1, b], tp=mate))

    def stage_c(b):
        arrived(xbuf.at[b, mate], pr.at[0, b])
        arrived(xbuf.at[b, diagonal], pr.at[1, b])

    def compute(b):
        total = jnp.zeros((rows, 1), f32)
        for q in range(n_q):
            v = xbuf[b, q].astype(f32)
            total += jnp.sum(v * v, axis=1, keepdims=True)
        scale = lax.rsqrt(total / (n_q * fb) + eps)
        for q in range(n_q):
            g = gain[:, q * fb:(q + 1) * fb].astype(f32)
            xn[:, q * fb:(q + 1) * fb] = (xbuf[b, q].astype(f32) * scale * g).astype(bf16)
        x = xn[...]
        gate = jnp.minimum(jnp.dot(x, wgb[...], preferred_element_type=f32), 7.0)
        up = jnp.clip(jnp.dot(x, wub[...], preferred_element_type=f32), -7.0, 7.0)
        act = (gate * jax.nn.sigmoid(1.702 * gate) * (up + 1.0)).astype(bf16)

        def down(q):
            cols = pl.ds(pl.multiple_of(q * fb, fb), fb)
            part[b, q] = jnp.dot(act, wdb[:, cols], preferred_element_type=f32).astype(bf16)

        for h in range(2):
            down(2 * h + 1 - c)
            push(remote(part.at[b, 2 * h + 1 - c], drecv.at[b, h], ds.at[b, h], dr.at[b, h], tp=mate))
        for h in range(2):
            down(2 * h + c)

    def stage_d(b):
        arrived(drecv.at[b, 1 - half], dr.at[b, 1 - half])
        esend[b] = (part[b, across].astype(f32) + drecv[b, 1 - half].astype(f32)).astype(bf16)
        push(remote(esend.at[b], erecv.at[b], es.at[b], er.at[b], tp=across))

    def stage_e(b, home):
        arrived(drecv.at[b, half], dr.at[b, half])
        arrived(erecv.at[b], er.at[b])
        value = (
            part[b, p].astype(f32) + drecv[b, half].astype(f32) + erecv[b].astype(f32)
        ).astype(bf16)
        if home:
            ret[z] = value
        else:
            fin[b] = value
            push(remote(fin.at[b], ret.at[z], fs.at[b], fr.at[z], ep=b))

    for copy in weights:
        copy.wait()
    b0, b1, b2, b3 = order
    compute(b0)
    stage_a(b1)
    stage_d(b0)
    stage_b(b1)
    stage_a(b2)
    stage_c(b1)
    compute(b1)
    stage_e(b0, True)
    stage_d(b1)
    stage_b(b2)
    stage_a(b3)
    stage_c(b2)
    compute(b2)
    stage_e(b1, False)
    stage_d(b2)
    stage_b(b3)
    stage_c(b3)
    compute(b3)
    stage_e(b2, False)
    stage_d(b3)
    stage_e(b3, False)

    def weighted(e):
        value = ret[e].astype(f32)
        total = jnp.zeros_like(value)
        for k in range(ids.shape[1]):
            total += jnp.where(ids[:, k:k + 1] == e, value * rw[:, k:k + 1], 0.0)
        return total

    combined = weighted(b0)
    for b in order[1:]:
        arrived(ret.at[b], fr.at[b])
        combined += weighted(b)
    sums = jnp.sum(combined * combined, axis=1, keepdims=True)
    sq[p] = jnp.transpose(jnp.broadcast_to(sums, (rows, 128)))[:8]
    for peer, k in ((mate, 0), (across, 1), (diagonal, 2)):
        push(remote(sq.at[p], sq.at[p], qs.at[k], qr.at[p], tp=peer))
    for peer in (mate, across, diagonal):
        arrived(sq.at[peer], qr.at[peer])
    squares = jnp.transpose(sq[0] + sq[1] + sq[2] + sq[3])[:, :1]
    scale = lax.rsqrt(squares / (n_q * fb) + eps)
    out[...] = (combined * scale * og[...].astype(f32)).astype(bf16)
    for copy in sends:
        copy.wait_send()


def fused(tokens, in_gain, expert_ids, route_weights, gate_weight, up_weight, down_weight, out_gain):
    n_ep, n_tp = lax.axis_size("ep"), lax.axis_size("tp")
    rows, width = tokens.shape
    hidden = gate_weight.shape[2]
    fb = width // n_tp
    vmem = pl.BlockSpec(memory_space=pltpu.VMEM)
    hbm = pl.BlockSpec(memory_space=pl.ANY)
    sem = pltpu.SemaphoreType.DMA
    piece = (rows, fb)
    return pl.pallas_call(
        layer_kernel,
        out_shape=jax.ShapeDtypeStruct(piece, bf16),
        in_specs=[hbm, vmem, vmem, vmem, hbm, hbm, hbm, vmem],
        out_specs=vmem,
        scratch_shapes=[
            pltpu.VMEM((n_ep, n_tp) + piece, bf16),
            pltpu.VMEM((width, hidden), bf16),
            pltpu.VMEM((width, hidden), bf16),
            pltpu.VMEM((hidden, width), bf16),
            pltpu.VMEM((rows, width), bf16),
            pltpu.VMEM((n_ep, n_tp) + piece, bf16),
            pltpu.VMEM((n_ep, 2) + piece, bf16),
            pltpu.VMEM((n_ep,) + piece, bf16),
            pltpu.VMEM((n_ep,) + piece, bf16),
            pltpu.VMEM((n_ep,) + piece, bf16),
            pltpu.VMEM((n_ep,) + piece, bf16),
            pltpu.VMEM((n_tp, 8, rows), f32),
            sem((n_tp + 3,)),
            sem((n_ep,)), sem((n_ep,)),
            sem((n_ep,)), sem((n_ep,)),
            sem((2, n_ep)), sem((2, n_ep)),
            sem((n_ep, 2)), sem((n_ep, 2)),
            sem((n_ep,)), sem((n_ep,)),
            sem((n_ep,)), sem((n_ep,)),
            sem((3,)), sem((n_tp,)),
        ],
        compiler_params=pltpu.CompilerParams(
            collective_id=0, has_side_effects=True, vmem_limit_bytes=60 * 1024 * 1024
        ),
        name="layer",
    )(
        tokens, in_gain.reshape(1, -1), expert_ids, route_weights,
        gate_weight, up_weight, down_weight, out_gain.reshape(1, -1),
    )


def on_device(
    tokens, in_gain, expert_ids, route_weights, gate_weight, up_weight, down_weight, out_gain
):
    n_ep = lax.axis_size("ep")
    n_tp = lax.axis_size("tp")
    tok_count, width = tokens.shape
    top_count = expert_ids.shape[1]
    experts = n_ep * gate_weight.shape[0]
    capacity = 2 * tok_count * top_count // experts
    if capacity >= tok_count and n_ep == 4 and n_tp == 4 and gate_weight.shape[0] == 1:
        return fused(
            tokens, in_gain, expert_ids, route_weights,
            gate_weight, up_weight, down_weight, out_gain,
        )
    feat_block = width // n_tp
    xf = tokens.astype(jnp.float32)
    normed_in = (
        xf * lax.rsqrt(jnp.mean(xf * xf, axis=1, keepdims=True) + eps) * in_gain.astype(jnp.float32)
    ).astype(jnp.bfloat16)
    flat_ids = expert_ids.reshape(-1)
    onehot = (flat_ids[:, None] == jnp.arange(experts, dtype=jnp.int32)[None, :]).astype(jnp.int32)
    slot = jnp.sum((jnp.cumsum(onehot, axis=0) - onehot) * onehot, axis=1)
    dest = flat_ids * capacity + slot
    token_of = jnp.arange(tok_count * top_count, dtype=jnp.int32) // top_count
    slot_token = jnp.full((experts * capacity,), tok_count, jnp.int32).at[dest].set(token_of)
    source = lax.dynamic_slice_in_dim(normed_in, lax.axis_index("tp") * feat_block, feat_block, 1)
    extended = jnp.concatenate([source, jnp.zeros((1, source.shape[1]), jnp.bfloat16)], axis=0)
    outgoing = extended[slot_token].reshape(experts, capacity, source.shape[1])
    w_gate = gate_weight[0]
    w_up = up_weight[0]
    arrived = lax.all_to_all(outgoing, "ep", split_axis=0, concat_axis=0, tiled=True).reshape(
        n_ep * capacity, feat_block
    )
    piece = lax.all_gather(arrived, "tp", axis=1, tiled=True)
    gate_pre = jnp.dot(piece, w_gate, preferred_element_type=jnp.float32)
    up_pre = jnp.dot(piece, w_up, preferred_element_type=jnp.float32)
    clamped = jnp.minimum(gate_pre, 7.0)
    bounded = jnp.clip(up_pre, -7.0, 7.0)
    act = (clamped * jax.nn.sigmoid(1.702 * clamped) * (bounded + 1.0)).astype(jnp.bfloat16)
    w_down = down_weight[0]
    summed = lax.psum_scatter(
        lax.dot_general(
            w_down, act, (((0,), (1,)), ((), ())), preferred_element_type=jnp.float32
        ).astype(jnp.bfloat16),
        "tp",
        scatter_dimension=0,
        tiled=True,
    )
    summed = summed.reshape(feat_block, n_ep, capacity)
    returned = lax.all_to_all(summed, "ep", split_axis=1, concat_axis=1, tiled=True)
    returned = returned.reshape(feat_block, experts * capacity).T
    picked = returned[dest].astype(jnp.float32).reshape(tok_count, top_count, feat_block)
    combined = jnp.sum(picked * route_weights[:, :, None], axis=1)
    squares = lax.psum(jnp.sum(combined * combined, axis=1), "tp")
    scale = lax.rsqrt(squares / width + eps)
    return (combined * scale[:, None] * out_gain.astype(jnp.float32)).astype(jnp.bfloat16)


def solution(mesh):
    placed = (
        P(("grp", "ep"), None),
        P(),
        P(("grp", "ep"), None),
        P(("grp", "ep"), None),
        P("ep", None, "tp"),
        P("ep", None, "tp"),
        P("ep", "tp", None),
        P("tp"),
    )
    return jax.shard_map(
        on_device, mesh=mesh, in_specs=placed, out_specs=P(("grp", "ep"), "tp"), check_vma=False
    )
```

profile of v0, /device:TPU:0, one launch (start us, length us, event | category | flops | bytes accessed | tf_op | source)
XLA Modules:
  0.0 84.7 jit_solution(7383297088223288387)
XLA Ops:
  0.0 1.2 %reshape.7.og = bf16[1,512]{1,0:T(2,128)(2,1)} reshape(bf16[512]{0:T(512)(128)(2,1)} %param.15) | data formatting | bytes 2048 | tf_op jit(solution)/shard_map/reshape | solution.py:212
  1.2 1.3 %reshape.6.gain = bf16[1,2048]{1,0:T(2,128)(2,1)} reshape(bf16[2048]{0:T(1024)(128)(2,1)} %param.9) | data formatting | bytes 8192 | tf_op jit(solution)/shard_map/reshape | solution.py:211
  2.5 1.5 %copy.9.ids = s32[256,2]{1,0:T(8,128)} copy(s32[256,2]{0,1:T(2,128)} %param.10) | data formatting | bytes 4096 | tf_op args[2]
  4.0 1.5 %copy.10.rw = f32[256,2]{1,0:T(8,128)} copy(f32[256,2]{0,1:T(2,128)} %param.11) | data formatting | bytes 4096 | tf_op args[3]
  5.5 77.6 %layer.1 = bf16[256,512]{1,0:T(8,128)(2,1)} custom-call(bf16[256,2048]{1,0:T(8,128)(2,1)} %tok.1, bf16[1,2048]{1,0:T(2,128)(2,1)} %reshape.6.gain, s32[256,2]{1,0:T(8,128)} %copy.9.ids, f32[256,2]{1,0:T(8,128)} %copy.10.rw, bf16[1,2048,512]{2,1,0:T(8,128)(2,1)} %wg.1, bf16[1,2048,512]{2,1,0:T(8,128)(2,1)} %wu.1, bf16[1,512,2048]{2,1,0:T(8,128)(2,1)} %wd.1, ...), custom_call_target="tpu_custom_call" | custom-call | tf_op jit(solution)/shard_map/layer/pallas_call | solution.py:179
  83.1 1.7 %copy.12 = bf16[256,512]{1,0:T(8,128)(2,1)} copy(bf16[256,512]{1,0:T(8,128)(2,1)} %layer.1) | data formatting | bytes 524288
where the time goes:
time: 85 us; the launch traced here: 84.7 us
  Pallas kernels  77.6 us (91%)
  local copies, waits for them, and re-layouts  7.15 us (8%)
    pallas_call x1, Pallas kernels, fused(): pl.pallas_call(layer_kernel, out_shape=jax.ShapeDtypeStruct(piece, bf16),...  77.6 us
    unnamed x3, local copies, waits for them, and re-layouts  4.62 us

commit v1 on v0

v1 whole, which is shorter than its diff:
```python
import jax
import jax.numpy as jnp
from jax import lax
from jax.experimental import pallas as pl
from jax.experimental.pallas import tpu as pltpu
from jax.sharding import PartitionSpec as P

eps = 1e-05
f32 = jnp.float32
bf16 = jnp.bfloat16
pieces = 2
lanes = 128

whole_in = (1, )
whole_out = (0, 1, )

send_order = (
    (
        (2, 0), (3, 0), (1, 0), (1, 1), (2, 1), (3, 1),
    ),
    (
        (2, 0), (1, 0), (3, 0), (1, 1), (3, 1), (2, 1),
    ),
)

schedule = (
    ("C", 0, 1), ("Z", 3, 0), ("C", 0, 0), ("Z", 1, 0), ("X", 3, 0), ("C", 3, 0),
    ("Z", 2, 0), ("P", 3, 0), ("X", 1, 0), ("C", 1, 0), ("Z", 1, 1), ("X", 2, 0),
    ("Z", 3, 1), ("P", 1, 0), ("X", 1, 1), ("C", 2, 0), ("P", 2, 0), ("Q", 3, 0),
    ("C", 1, 1), ("Z", 2, 1), ("Q", 1, 0), ("X", 3, 1), ("C", 3, 1), ("Q", 2, 0),
    ("P", 3, 1), ("X", 2, 1), ("C", 2, 1), ("P", 1, 1), ("P", 2, 1), ("Q", 3, 1),
    ("P", 0, 1), ("Q", 1, 1), ("P", 0, 0), ("Q", 2, 1), ("Q", 0, 1), ("Q", 0, 0),
)


def layer_kernel(
    tok, gain, ids, rw, wg, wu, wd, og, out,
    raw, xbuf, wgb, wub, wdb, g32, share, part, drecv, esend, erecv, brecv, fin, ret, acc, sq,
    ts, ws, zs, zr, bs, br, ys, yr, xs, xr, ps, pr, ds, dr, es, er, fs, fr, qs, qr,
):
    z, p = lax.axis_index("ep"), lax.axis_index("tp")
    n_ep, n_q, rows, fb = xbuf.shape
    part_rows = rows // pieces
    half, c = p // 2, p % 2
    mate = half * 2 + 1 - c
    across = (1 - half) * 2 + c
    diagonal = (1 - half) * 2 + 1 - c
    hi = z // 2
    order = (z, 1 - z + hi * 4, 2 - hi, 3 - 3 * hi)
    middle = jnp.logical_or(z == 1, z == 2)

    def span(h):
        return pl.ds(h * part_rows, part_rows)

    def remote(src, dst, s, r, **where):
        return pltpu.make_async_remote_copy(
            src_ref=src, dst_ref=dst, send_sem=s, recv_sem=r,
            device_id=where, device_id_type=pl.DeviceIdType.MESH,
        )

    def signal(**where):
        pl.semaphore_signal(barrier, inc=1, device_id=where, device_id_type=pl.DeviceIdType.MESH)

    loads = [
        [
            pltpu.make_async_copy(
                tok.at[span(h), pl.ds(q * fb, fb)], raw.at[q, span(h)], ts.at[h, q]
            )
            for q in range(n_q)
        ]
        for h in range(pieces)
    ]
    weights = [
        pltpu.make_async_copy(wg.at[0], wgb, ws.at[0]),
        pltpu.make_async_copy(wu.at[0], wub, ws.at[1]),
    ] + [
        pltpu.make_async_copy(wd.at[0, :, pl.ds(q * fb, fb)], wdb.at[q], ws.at[2 + q])
        for q in range(n_q)
    ]
    barrier = pltpu.get_barrier_semaphore()
    for peer in (mate, across, diagonal):
        signal(tp=peer)
    for b in order[1:]:
        signal(ep=b)
    for copy in sum(loads, []) + weights:
        copy.start()
    for q in range(n_q):
        g32[q] = gain[q * (fb // lanes):(q + 1) * (fb // lanes), :].astype(f32)
    share[...] = jnp.transpose(jnp.concatenate(
        [
            sum(jnp.where(ids[k:k + 1, :] == e, rw[k:k + 1, :], 0.0) for k in range(ids.shape[0]))
            for e in order
        ]
        + [jnp.zeros((lanes - len(order), rows), f32)],
        axis=0,
    ))

    sends = []

    def push(copy):
        copy.start()
        sends.append(copy)

    def scaled(value, i, r):
        w = share[r, i:i + 1]
        return jnp.where(w != 0.0, value * w, 0.0)

    def normalize(h):
        for copy in loads[h]:
            copy.wait()
        total = jnp.zeros((part_rows, 1), f32)
        for q in range(n_q):
            v = raw[q, span(h)].astype(f32)
            total += jnp.sum(v * v, axis=1, keepdims=True)
        scale = lax.rsqrt(total / (n_q * fb) + eps)

        def one(q):
            for j in range(fb // lanes):
                cols = slice(j * lanes, (j + 1) * lanes)
                g = g32[q][j:j + 1, :]
                xbuf[z, q, span(h), cols] = (
                    raw[q, span(h), cols].astype(f32) * scale * g
                ).astype(bf16)

        one(p)
        if h in whole_in:
            one(across)
        if h == 0:
            pl.semaphore_wait(barrier, 6)
        mine, other = xbuf.at[z, p, span(h)], xbuf.at[z, across, span(h)]
        first = {
            i: [remote(mine, mine, zs.at[i, h], zr.at[z, h], ep=order[i])] for i in (1, 2, 3)
        }
        if h in whole_in:
            first[1].append(remote(other, other, ys.at[h], yr.at[h], ep=order[1]))
        ends, middles = (tuple(i for i, k in o if k == h) for o in send_order)

        def start(places):
            for i in places:
                for copy in first[i]:
                    copy.start()

        if ends == middles:
            start(ends)
        else:
            pl.when(middle)(lambda: start(middles))
            pl.when(jnp.logical_not(middle))(lambda: start(ends))
        sends.extend(sum(first.values(), []))
        for q in (mate, diagonal) if h in whole_in else (across, mate, diagonal):
            one(q)

    def arrived(ref, sem):
        pltpu.make_async_copy(ref, ref, sem).wait()

    def stage_z(i, h):
        b = order[i]
        piece = xbuf.at[b, p, span(h)]
        arrived(piece, zr.at[b, h])
        if i > 1 or h not in whole_in:
            push(remote(piece, piece, xs.at[b, h], xr.at[b, h], tp=across))
        push(remote(piece, piece, ps.at[0, b, h], pr.at[0, b, h], tp=mate))

    def stage_x(i, h):
        b = order[i]
        piece = xbuf.at[b, across, span(h)]
        arrived(piece, yr.at[h] if i == 1 and h in whole_in else xr.at[b, h])
        push(remote(piece, piece, ps.at[1, b, h], pr.at[1, b, h], tp=mate))

    def stage_c(i, h):
        b = order[i]
        if i > 0:
            arrived(xbuf.at[b, mate, span(h)], pr.at[0, b, h])
            arrived(xbuf.at[b, diagonal, span(h)], pr.at[1, b, h])
        elif (i, h) == own_first:
            for copy in weights:
                copy.wait()
        x = jnp.concatenate([xbuf[b, q, span(h)] for q in range(n_q)], axis=1)
        gate = jnp.minimum(jnp.dot(x, wgb[...], preferred_element_type=f32), 7.0)
        up = jnp.clip(jnp.dot(x, wub[...], preferred_element_type=f32), -7.0, 7.0)
        act = (gate * jax.nn.sigmoid(1.702 * gate) * (up + 1.0)).astype(bf16)

        def down(q):
            part[b, q, span(h)] = jnp.dot(
                act, wdb[q], preferred_element_type=f32
            ).astype(bf16)

        for s in range(2):
            q = 2 * s + 1 - c
            down(q)
            push(remote(
                part.at[b, q, span(h)], drecv.at[b, s, span(h)],
                ds.at[b, s, h], dr.at[b, s, h], tp=mate,
            ))
        for s in range(2):
            down(2 * s + c)

    def stage_p(i, h):
        b, r = order[i], span(h)
        arrived(drecv.at[b, 1 - half, r], dr.at[b, 1 - half, h])
        value = part[b, across, r].astype(f32) + drecv[b, 1 - half, r].astype(f32)
        if i == 0:
            value = scaled(value, 0, r)
            if h in whole_out:
                arrived(brecv.at[r], br.at[h])
                value += scaled(brecv[r].astype(f32), 1, r)
        esend[b, r] = value.astype(bf16)
        if i == 1 and h in whole_out:
            push(remote(esend.at[b, r], brecv.at[r], bs.at[h], br.at[h], ep=b))
        else:
            push(remote(esend.at[b, r], erecv.at[b, r], es.at[b, h], er.at[b, h], tp=across))

    def stage_q(i, h):
        b, r = order[i], span(h)
        arrived(drecv.at[b, half, r], dr.at[b, half, h])
        value = part[b, p, r].astype(f32) + drecv[b, half, r].astype(f32)
        if i == 0:
            value = scaled(value, 0, r)
        if i != 1 or h not in whole_out:
            arrived(erecv.at[b, r], er.at[b, h])
            value += erecv[b, r].astype(f32)
        if i == 0:
            acc[r] = value
        else:
            fin[b, r] = value.astype(bf16)
            push(remote(fin.at[b, r], ret.at[z, r], fs.at[b, h], fr.at[z, h], ep=b))

    for h in range(pieces):
        with jax.named_scope(f"N{h}"):
            normalize(h)
    own_first = next(s[1:] for s in schedule if s[0] == "C")
    stages = {"Z": stage_z, "X": stage_x, "C": stage_c, "P": stage_p, "Q": stage_q}
    for name, i, h in schedule:
        with jax.named_scope(f"{name}{i}{h}"):
            stages[name](i, h)

    with jax.named_scope("comb"):
        sums = []
        for h in range(pieces):
            r = span(h)
            combined = acc[r]
            for i in (1, 2, 3):
                arrived(ret.at[order[i], r], fr.at[order[i], h])
                combined += scaled(ret[order[i], r].astype(f32), i, r)
            acc[r] = combined
            sums.append(jnp.sum(combined * combined, axis=1, keepdims=True))
        sums = jnp.concatenate(sums, axis=0)
        sq[p] = jnp.transpose(jnp.broadcast_to(sums, (rows, lanes)))[:8]
    for peer, k in ((mate, 0), (across, 1), (diagonal, 2)):
        push(remote(sq.at[p], sq.at[p], qs.at[k], qr.at[p], tp=peer))
    with jax.named_scope("sqw"):
        for peer in (mate, across, diagonal):
            arrived(sq.at[peer], qr.at[peer])
    with jax.named_scope("out"):
        squares = jnp.transpose(sq[0] + sq[1] + sq[2] + sq[3])[:, :1]
        scale = lax.rsqrt(squares / (n_q * fb) + eps)
        og32 = og[...].astype(f32)
        for j in range(fb // lanes):
            cols = slice(j * lanes, (j + 1) * lanes)
            out[:, cols] = (acc[:, cols] * scale * og32[j:j + 1, :]).astype(bf16)
    for copy in sends:
        copy.wait_send()


def fused(tokens, in_gain, expert_ids, route_weights, gate_weight, up_weight, down_weight, out_gain):
    n_ep, n_tp = lax.axis_size("ep"), lax.axis_size("tp")
    rows, width = tokens.shape
    hidden = gate_weight.shape[2]
    fb = width // n_tp
    vmem = pl.BlockSpec(memory_space=pltpu.VMEM)
    hbm = pl.BlockSpec(memory_space=pl.ANY)
    sem = pltpu.SemaphoreType.DMA
    piece = (rows, fb)
    return pl.pallas_call(
        layer_kernel,
        out_shape=jax.ShapeDtypeStruct(piece, bf16),
        in_specs=[hbm, vmem, vmem, vmem, hbm, hbm, hbm, vmem],
        out_specs=vmem,
        scratch_shapes=[
            pltpu.VMEM((n_tp,) + piece, bf16),
            pltpu.VMEM((n_ep, n_tp) + piece, bf16),
            pltpu.VMEM((width, hidden), bf16),
            pltpu.VMEM((width, hidden), bf16),
            pltpu.VMEM((n_tp, hidden, fb), bf16),
            pltpu.VMEM((n_tp, fb // lanes, lanes), f32),
            pltpu.VMEM((rows, lanes), f32),
            pltpu.VMEM((n_ep, n_tp) + piece, bf16),
            pltpu.VMEM((n_ep, 2) + piece, bf16),
            pltpu.VMEM((n_ep,) + piece, bf16),
            pltpu.VMEM((n_ep,) + piece, bf16),
            pltpu.VMEM(piece, bf16),
            pltpu.VMEM((n_ep,) + piece, bf16),
            pltpu.VMEM((n_ep,) + piece, bf16),
            pltpu.VMEM(piece, f32),
            pltpu.VMEM((n_tp, 8, rows), f32),
            sem((pieces, n_tp)), sem((2 + n_tp,)),
            sem((4, pieces)), sem((n_ep, pieces)),
            sem((pieces,)), sem((pieces,)),
            sem((pieces,)), sem((pieces,)),
            sem((n_ep, pieces)), sem((n_ep, pieces)),
            sem((2, n_ep, pieces)), sem((2, n_ep, pieces)),
            sem((n_ep, 2, pieces)), sem((n_ep, 2, pieces)),
            sem((n_ep, pieces)), sem((n_ep, pieces)),
            sem((n_ep, pieces)), sem((n_ep, pieces)),
            sem((3,)), sem((n_tp,)),
        ],
        compiler_params=pltpu.CompilerParams(
            collective_id=0, has_side_effects=True, vmem_limit_bytes=60 * 1024 * 1024
        ),
        name="layer",
    )(
        tokens, in_gain.reshape(-1, lanes), expert_ids.T, route_weights.T,
        gate_weight, up_weight, down_weight, out_gain.reshape(-1, lanes),
    )


def on_device(
    tokens, in_gain, expert_ids, route_weights, gate_weight, up_weight, down_weight, out_gain
):
    n_ep = lax.axis_size("ep")
    n_tp = lax.axis_size("tp")
    tok_count, width = tokens.shape
    top_count = expert_ids.shape[1]
    experts = n_ep * gate_weight.shape[0]
    capacity = 2 * tok_count * top_count // experts
    if capacity >= tok_count and n_ep == 4 and n_tp == 4 and gate_weight.shape[0] == 1:
        return fused(
            tokens, in_gain, expert_ids, route_weights,
            gate_weight, up_weight, down_weight, out_gain,
        )
    feat_block = width // n_tp
    xf = tokens.astype(jnp.float32)
    normed_in = (
        xf * lax.rsqrt(jnp.mean(xf * xf, axis=1, keepdims=True) + eps) * in_gain.astype(jnp.float32)
    ).astype(jnp.bfloat16)
    flat_ids = expert_ids.reshape(-1)
    onehot = (flat_ids[:, None] == jnp.arange(experts, dtype=jnp.int32)[None, :]).astype(jnp.int32)
    slot = jnp.sum((jnp.cumsum(onehot, axis=0) - onehot) * onehot, axis=1)
    dest = flat_ids * capacity + slot
    token_of = jnp.arange(tok_count * top_count, dtype=jnp.int32) // top_count
    slot_token = jnp.full((experts * capacity,), tok_count, jnp.int32).at[dest].set(token_of)
    source = lax.dynamic_slice_in_dim(normed_in, lax.axis_index("tp") * feat_block, feat_block, 1)
    extended = jnp.concatenate([source, jnp.zeros((1, source.shape[1]), jnp.bfloat16)], axis=0)
    outgoing = extended[slot_token].reshape(experts, capacity, source.shape[1])
    w_gate = gate_weight[0]
    w_up = up_weight[0]
    arrived = lax.all_to_all(outgoing, "ep", split_axis=0, concat_axis=0, tiled=True).reshape(
        n_ep * capacity, feat_block
    )
    piece = lax.all_gather(arrived, "tp", axis=1, tiled=True)
    gate_pre = jnp.dot(piece, w_gate, preferred_element_type=jnp.float32)
    up_pre = jnp.dot(piece, w_up, preferred_element_type=jnp.float32)
    clamped = jnp.minimum(gate_pre, 7.0)
    bounded = jnp.clip(up_pre, -7.0, 7.0)
    act = (clamped * jax.nn.sigmoid(1.702 * clamped) * (bounded + 1.0)).astype(jnp.bfloat16)
    w_down = down_weight[0]
    summed = lax.psum_scatter(
        lax.dot_general(
            w_down, act, (((0,), (1,)), ((), ())), preferred_element_type=jnp.float32
        ).astype(jnp.bfloat16),
        "tp",
        scatter_dimension=0,
        tiled=True,
    )
    summed = summed.reshape(feat_block, n_ep, capacity)
    returned = lax.all_to_all(summed, "ep", split_axis=1, concat_axis=1, tiled=True)
    returned = returned.reshape(feat_block, experts * capacity).T
    picked = returned[dest].astype(jnp.float32).reshape(tok_count, top_count, feat_block)
    combined = jnp.sum(picked * route_weights[:, :, None], axis=1)
    squares = lax.psum(jnp.sum(combined * combined, axis=1), "tp")
    scale = lax.rsqrt(squares / width + eps)
    return (combined * scale[:, None] * out_gain.astype(jnp.float32)).astype(jnp.bfloat16)


def solution(mesh):
    placed = (
        P(("grp", "ep"), None),
        P(),
        P(("grp", "ep"), None),
        P(("grp", "ep"), None),
        P("ep", None, "tp"),
        P("ep", None, "tp"),
        P("ep", "tp", None),
        P("tp"),
    )
    return jax.shard_map(
        on_device, mesh=mesh, in_specs=placed, out_specs=P(("grp", "ep"), "tp"), check_vma=False
    )
```

time: 85 us -> 61.3 us (0.72)
  Pallas kernels: 77.6 us -> 59.5 us
  local copies, waits for them, and re-layouts: 7.15 us -> 1.67 us
    pallas_call x1, Pallas kernels: 77.6 us -> 59.5 us  [fused(): pl.pallas_call(layer_kernel, out_shape=jax.ShapeDtypeStruct(piece, bf16),...]
    unnamed x3 -> x1, local copies, waits for them, and re-layouts: 4.62 us -> 1.67 us
    reshape x2 -> x0, local copies, waits for them, and re-layouts: 2.53 us -> none  [the longest x1 1.29 us: fused(): in_gain.reshape(1, -1)]
where the time goes in v1:
time: 61.3 us; the launch traced here: 61.2 us
  Pallas kernels  59.5 us (97%)
  local copies, waits for them, and re-layouts  1.67 us (3%)
    pallas_call x1, Pallas kernels, fused(): pl.pallas_call(layer_kernel, out_shape=jax.ShapeDtypeStruct(piece, bf16),...  59.5 us
    unnamed x1, local copies, waits for them, and re-layouts  1.67 us

profile of v1, /device:TPU:0, one launch (start us, length us, event | category | flops | bytes accessed | tf_op | source)
XLA Modules:
  0.0 61.2 jit_solution(9794674567422786845)
XLA Ops:
  0.0 59.5 %layer.1 = bf16[256,512]{1,0:T(8,128)(2,1)} custom-call(bf16[256,2048]{1,0:T(8,128)(2,1)} %tok.1, bf16[16,128]{1,0:T(8,128)(2,1)} %bitcast.4, s32[2,256]{1,0:T(2,128)} %bitcast.5, f32[2,256]{1,0:T(2,128)} %bitcast.6, bf16[1,2048,512]{2,1,0:T(8,128)(2,1)} %wg.1, bf16[1,2048,512]{2,1,0:T(8,128)(2,1)} %wu.1, bf16[1,512,2048]{2,1,0:T(8,128)(2,1)} %wd.1, ...), custom_call_target="tpu_custom_call" | custom-call | tf_op jit(solution)/shard_map/layer/pallas_call | solution.py:273
  59.5 1.7 %copy.10 = bf16[256,512]{1,0:T(8,128)(2,1)} copy(bf16[256,512]{1,0:T(8,128)(2,1)} %layer.1) | data formatting | bytes 524288

commit v2 on v0

v2 whole, which is shorter than its diff:
```python
import jax
import jax.numpy as jnp
from jax import lax
from jax.experimental import pallas as pl
from jax.experimental.pallas import tpu as pltpu
from jax.sharding import PartitionSpec as P

eps = 1e-05
f32 = jnp.float32
bf16 = jnp.bfloat16
pieces = 2
lanes = 128

whole_in = ()
whole_out = (0, 1, )

forwarded = (2, 3)

send_order = (
    (
        (2, 0), (1, 0), (2, 1), (1, 1),
    ),
    (
        (2, 0), (1, 0), (2, 1), (1, 1),
    ),
)

schedules = (
    (
        ("C", 0, 1), ("Z", 1, 0), ("C", 0, 0), ("Z", 1, 1), ("X", 1, 0), ("Z", 3, 0),
        ("C", 1, 0), ("X", 1, 1), ("Z", 2, 0), ("P", 1, 0), ("Q", 1, 0), ("Z", 3, 1),
        ("C", 1, 1), ("X", 2, 0), ("P", 1, 1), ("X", 3, 0), ("Z", 2, 1), ("C", 2, 0),
        ("X", 3, 1), ("P", 2, 0), ("Q", 1, 1), ("C", 3, 0), ("P", 3, 0), ("X", 2, 1),
        ("C", 3, 1), ("Q", 2, 0), ("P", 3, 1), ("C", 2, 1), ("Q", 3, 0), ("P", 2, 1),
        ("Q", 3, 1), ("P", 0, 0), ("P", 0, 1), ("Q", 2, 1), ("Q", 0, 1), ("R", 0, 1),
        ("Q", 0, 0), ("R", 0, 0), ("O", 0, 1), ("O", 0, 0),
    ),
    (
        ("C", 0, 0), ("Z", 3, 0), ("Z", 2, 0), ("Z", 3, 1), ("C", 0, 1), ("X", 2, 0),
        ("Z", 1, 1), ("X", 3, 0), ("Z", 2, 1), ("C", 2, 0), ("X", 3, 1), ("C", 3, 1),
        ("Z", 1, 0), ("P", 2, 0), ("P", 0, 0), ("X", 1, 1), ("C", 3, 0), ("C", 1, 1),
        ("P", 3, 0), ("P", 1, 1), ("Q", 1, 1), ("X", 2, 1), ("P", 3, 1), ("X", 1, 0),
        ("C", 1, 0), ("P", 1, 0), ("C", 2, 1), ("Q", 2, 0), ("Q", 3, 0), ("P", 2, 1),
        ("P", 0, 1), ("Q", 1, 0), ("Q", 3, 1), ("Q", 2, 1), ("Q", 0, 1), ("Q", 0, 0),
        ("R", 0, 0), ("R", 0, 1), ("O", 0, 0), ("O", 0, 1),
    ),
)


def layer_kernel(
    tok, gain_in, ids_in, rw_in, wg, wu, wd, og_in, out,
    gain, ids, rw, og, raw, xbuf, wgu, wdb, g32, table, far_table, share, part, drecv, esend, erecv, brecv, fin,
    mrecv, ret, acc, sq,
    ms, ts, ws, hs, hr, zs, zr, vs, bs, br, ys, yr, xs, xr, ps, pr, ds, dr, es, er, fs, fr, mr, qs, qr,
):
    z, p = lax.axis_index("ep"), lax.axis_index("tp")
    n_ep, n_q, rows, fb = xbuf.shape
    part_rows, hidden = rows // pieces, wg.shape[2]
    half, c = p // 2, p % 2
    mate = half * 2 + 1 - c
    across = (1 - half) * 2 + c
    diagonal = (1 - half) * 2 + 1 - c
    hi = z // 2
    order = (z, 1 - z + hi * 4, 2 - hi, 3 - 3 * hi)
    middle = jnp.logical_or(z == 1, z == 2)

    def span(h):
        return pl.ds(h * part_rows, part_rows)

    def remote(src, dst, s, r, **where):
        return pltpu.make_async_remote_copy(
            src_ref=src, dst_ref=dst, send_sem=s, recv_sem=r,
            device_id=where, device_id_type=pl.DeviceIdType.MESH,
        )

    def signal(**where):
        pl.semaphore_signal(barrier, inc=1, device_id=where, device_id_type=pl.DeviceIdType.MESH)

    loads = [
        [
            pltpu.make_async_copy(
                tok.at[span(h), pl.ds(q * fb, fb)], raw.at[q, span(h)], ts.at[h, q]
            )
            for q in range(n_q)
        ]
        for h in range(pieces)
    ]
    weights = [
        pltpu.make_async_copy(wg.at[0], wgu.at[:, :hidden], ws.at[0]),
        pltpu.make_async_copy(wu.at[0], wgu.at[:, hidden:], ws.at[1]),
    ] + [
        pltpu.make_async_copy(
            wd.at[0, :, pl.ds(q * fb, fb)],
            wdb.at[q % 2, :, pl.ds(q // 2 * fb, fb)], ws.at[2 + q],
        )
        for q in range(n_q)
    ]
    barrier = pltpu.get_barrier_semaphore()
    for peer in (mate, across, diagonal):
        signal(tp=peer)
    for b in order[1:]:
        signal(ep=b)
    small = [
        pltpu.make_async_copy(a, b, ms.at[k])
        for k, (a, b) in enumerate(((gain_in, gain), (ids_in, ids), (rw_in, rw), (og_in, og)))
    ]
    for copy in loads[0] + small + sum(loads[1:], []) + weights:
        copy.start()
    for copy in small:
        copy.wait()
    for q in range(n_q):
        g32[q] = gain[q * (fb // lanes):(q + 1) * (fb // lanes), :].astype(f32)
    for i, e in enumerate(order):
        row = sum(
            jnp.where(ids[k:k + 1, :] == e, rw[k:k + 1, :], 0.0) for k in range(ids.shape[0])
        )
        table[i] = jnp.broadcast_to(row, table.shape[1:])

    def columns(tables):
        rest = jnp.zeros((lanes - 8 * len(tables), rows), f32)
        return jnp.transpose(jnp.concatenate(tables + [rest], axis=0))

    share[0] = columns([table[0]])

    def pipeline(is_middle):
        sends = []

        def push(copy):
            copy.start()
            sends.append(copy)

        def normalize(h):
            for copy in loads[h]:
                copy.wait()
            total = jnp.zeros((part_rows, 1), f32)
            for q in range(n_q):
                v = raw[q, span(h)].astype(f32)
                total += jnp.sum(v * v, axis=1, keepdims=True)
            scale = lax.rsqrt(total / (n_q * fb) + eps)

            def one(q):
                for j in range(fb // lanes):
                    cols = slice(j * lanes, (j + 1) * lanes)
                    g = g32[q][j:j + 1, :]
                    xbuf[z, q, span(h), cols] = (
                        raw[q, span(h), cols].astype(f32) * scale * g
                    ).astype(bf16)

            one(p)
            if h in whole_in:
                one(across)
            if h == 0:
                pl.semaphore_wait(barrier, 6)
                for i in (1, 2, 3):
                    push(remote(table.at[i], far_table.at[z], hs.at[i], hr.at[z], ep=order[i]))
            mine, other = xbuf.at[z, p, span(h)], xbuf.at[z, across, span(h)]
            for i, k in send_order[is_middle]:
                if k == h:
                    push(remote(mine, mine, zs.at[i, h], zr.at[z, h], ep=order[i]))
                    if i == 1 and h in whole_in:
                        push(remote(other, other, ys.at[h], yr.at[h], ep=order[1]))
            for q in (mate, diagonal) if h in whole_in else (across, mate, diagonal):
                one(q)

        def arrived(ref, sem):
            pltpu.make_async_copy(ref, ref, sem).wait()

        def stage_z(i, h):
            b = order[i]
            piece = xbuf.at[b, p, span(h)]
            arrived(piece, zr.at[b, h])
            if i > 1 or h not in whole_in:
                push(remote(piece, piece, xs.at[b, h], xr.at[b, h], tp=across))
            if is_middle and i in forwarded:
                push(remote(piece, piece, vs.at[i, h], zr.at[b, h], ep=order[1]))
            push(remote(piece, piece, ps.at[0, b, h], pr.at[0, b, h], tp=mate))

        def stage_x(i, h):
            b = order[i]
            piece = xbuf.at[b, across, span(h)]
            arrived(piece, yr.at[h] if i == 1 and h in whole_in else xr.at[b, h])
            push(remote(piece, piece, ps.at[1, b, h], pr.at[1, b, h], tp=mate))

        def stage_c(i, h):
            b = order[i]
            if i > 0:
                arrived(xbuf.at[b, mate, span(h)], pr.at[0, b, h])
                arrived(xbuf.at[b, diagonal, span(h)], pr.at[1, b, h])
            if (i, h) == own_first:
                for copy in weights:
                    copy.wait()
            x = jnp.concatenate([xbuf[b, q, span(h)] for q in range(n_q)], axis=1)
            both = jnp.dot(x, wgu[...], preferred_element_type=f32)
            gate = jnp.minimum(both[:, :hidden], 7.0)
            up = jnp.clip(both[:, hidden:], -7.0, 7.0)
            if (i, h) == far_first:
                for e in order[1:]:
                    arrived(far_table.at[e], hr.at[e])
                share[1] = columns([far_table[e] for e in order[1:]])
            k = max(i - 1, 0) * 8
            w = share[min(i, 1), span(h), k:k + 1]
            act = (gate * jax.nn.sigmoid(1.702 * gate) * (up + 1.0) * w).astype(bf16)

            def down(parity):
                y = jnp.dot(act, wdb[parity], preferred_element_type=f32).astype(bf16)
                for k in range(2):
                    part[b, 2 * k + parity, span(h)] = y[:, k * fb:(k + 1) * fb]

            down(1 - c)
            for k in range(2):
                push(remote(
                    part.at[b, 2 * k + 1 - c, span(h)], drecv.at[b, k, span(h)],
                    ds.at[b, k, h], dr.at[b, k, h], tp=mate,
                ))
            down(c)

        def stage_p(i, h):
            b, r = order[i], span(h)
            arrived(drecv.at[b, 1 - half, r], dr.at[b, 1 - half, h])
            value = part[b, across, r].astype(f32) + drecv[b, 1 - half, r].astype(f32)
            if i == 0 and h in whole_out:
                arrived(brecv.at[r], br.at[h])
                value += brecv[r].astype(f32)
            esend[b, r] = value.astype(bf16)
            if i == 1 and h in whole_out:
                push(remote(esend.at[b, r], brecv.at[r], bs.at[h], br.at[h], ep=b))
            else:
                push(remote(esend.at[b, r], erecv.at[b, r], es.at[b, h], er.at[b, h], tp=across))

        def stage_q(i, h):
            b, r = order[i], span(h)
            arrived(drecv.at[b, half, r], dr.at[b, half, h])
            value = part[b, p, r].astype(f32) + drecv[b, half, r].astype(f32)
            if i != 1 or h not in whole_out:
                arrived(erecv.at[b, r], er.at[b, h])
                value += erecv[b, r].astype(f32)
            if i == 0:
                acc[r] = value
                return
            if is_middle and i > 1:
                arrived(mrecv.at[b, r], mr.at[b, h])
                value += mrecv[b, r].astype(f32)
            fin[b, r] = value.astype(bf16)
            if is_middle or i == 1:
                k = min(i, 2) - 1
                push(remote(fin.at[b, r], ret.at[k, r], fs.at[b, h], fr.at[k, h], ep=b))
            else:
                push(remote(fin.at[b, r], mrecv.at[b, r], fs.at[b, h], mr.at[b, h], ep=order[1]))

        def stage_r(i, h):
            r = span(h)
            for k in range(2):
                arrived(ret.at[k, r], fr.at[k, h])
            combined = acc[r] + ret[0, r].astype(f32) + ret[1, r].astype(f32)
            acc[r] = combined
            sums = jnp.sum(combined * combined, axis=1, keepdims=True)
            sq[p, h] = jnp.transpose(jnp.broadcast_to(sums, (part_rows, lanes)))[:8]
            for k, peer in enumerate((mate, across, diagonal)):
                push(remote(sq.at[p, h], sq.at[p, h], qs.at[k, h], qr.at[p, h], tp=peer))

        def stage_o(i, h):
            r = span(h)
            for peer in (mate, across, diagonal):
                arrived(sq.at[peer, h], qr.at[peer, h])
            squares = jnp.transpose(sq[0, h] + sq[1, h] + sq[2, h] + sq[3, h])[:, :1]
            scale = lax.rsqrt(squares / (n_q * fb) + eps)
            og32 = og[...].astype(f32)
            for j in range(fb // lanes):
                cols = slice(j * lanes, (j + 1) * lanes)
                out[r, cols] = (acc[r, cols] * scale * og32[j:j + 1, :]).astype(bf16)

        for h in range(pieces):
            with jax.named_scope(f"N{h}"):
                normalize(h)
        schedule = schedules[is_middle]
        own_first = next(s[1:] for s in schedule if s[0] == "C")
        far_first = next(s[1:] for s in schedule if s[0] == "C" and s[1] > 0)
        stages = {"Z": stage_z, "X": stage_x, "C": stage_c, "P": stage_p, "Q": stage_q}
        stages |= {"R": stage_r, "O": stage_o}
        for name, i, h in schedule:
            with jax.named_scope(f"{name}{i}{h}"):
                stages[name](i, h)
        for copy in sends:
            copy.wait_send()

    pl.when(middle)(lambda: pipeline(True))
    pl.when(jnp.logical_not(middle))(lambda: pipeline(False))


def fused(tokens, in_gain, expert_ids, route_weights, gate_weight, up_weight, down_weight, out_gain):
    n_ep, n_tp = lax.axis_size("ep"), lax.axis_size("tp")
    rows, width = tokens.shape
    hidden = gate_weight.shape[2]
    fb = width // n_tp
    hbm = pl.BlockSpec(memory_space=pl.ANY)
    sem = pltpu.SemaphoreType.DMA
    piece = (rows, fb)
    return pl.pallas_call(
        layer_kernel,
        out_shape=pltpu.VMEM(piece, bf16),
        in_specs=[hbm] * 8,
        out_specs=pl.BlockSpec(memory_space=pltpu.VMEM),
        scratch_shapes=[
            pltpu.VMEM((width // lanes, lanes), bf16),
            pltpu.VMEM(expert_ids.shape[::-1], jnp.int32),
            pltpu.VMEM(route_weights.shape[::-1], f32),
            pltpu.VMEM((fb // lanes, lanes), bf16),
            pltpu.VMEM((n_tp,) + piece, bf16),
            pltpu.VMEM((n_ep, n_tp) + piece, bf16),
            pltpu.VMEM((width, 2 * hidden), bf16),
            pltpu.VMEM((2, hidden, width // 2), bf16),
            pltpu.VMEM((n_tp, fb // lanes, lanes), f32),
            pltpu.VMEM((n_ep, 8, rows), f32),
            pltpu.VMEM((n_ep, 8, rows), f32),
            pltpu.VMEM((2, rows, lanes), f32),
            pltpu.VMEM((n_ep, n_tp) + piece, bf16),
            pltpu.VMEM((n_ep, 2) + piece, bf16),
            pltpu.VMEM((n_ep,) + piece, bf16),
            pltpu.VMEM((n_ep,) + piece, bf16),
            pltpu.VMEM(piece, bf16),
            pltpu.VMEM((n_ep,) + piece, bf16),
            pltpu.VMEM((n_ep,) + piece, bf16),
            pltpu.VMEM((2,) + piece, bf16),
            pltpu.VMEM(piece, f32),
            pltpu.VMEM((n_tp, pieces, 8, rows // pieces), f32),
            sem((4,)), sem((pieces, n_tp)), sem((2 + n_tp,)),
            sem((4,)), sem((n_ep,)),
            sem((4, pieces)), sem((n_ep, pieces)), sem((4, pieces)),
            sem((pieces,)), sem((pieces,)),
            sem((pieces,)), sem((pieces,)),
            sem((n_ep, pieces)), sem((n_ep, pieces)),
            sem((2, n_ep, pieces)), sem((2, n_ep, pieces)),
            sem((n_ep, 2, pieces)), sem((n_ep, 2, pieces)),
            sem((n_ep, pieces)), sem((n_ep, pieces)),
            sem((n_ep, pieces)), sem((2, pieces)), sem((n_ep, pieces)),
            sem((3, pieces)), sem((n_tp, pieces)),
        ],
        compiler_params=pltpu.CompilerParams(
            collective_id=0, has_side_effects=True, vmem_limit_bytes=60 * 1024 * 1024
        ),
        name="layer",
    )(
        tokens, in_gain.reshape(-1, lanes), expert_ids.T, route_weights.T,
        gate_weight, up_weight, down_weight, out_gain.reshape(-1, lanes),
    )


def on_device(
    tokens, in_gain, expert_ids, route_weights, gate_weight, up_weight, down_weight, out_gain
):
    n_ep = lax.axis_size("ep")
    n_tp = lax.axis_size("tp")
    tok_count, width = tokens.shape
    top_count = expert_ids.shape[1]
    experts = n_ep * gate_weight.shape[0]
    capacity = 2 * tok_count * top_count // experts
    if capacity >= tok_count and n_ep == 4 and n_tp == 4 and gate_weight.shape[0] == 1:
        return fused(
            tokens, in_gain, expert_ids, route_weights,
            gate_weight, up_weight, down_weight, out_gain,
        )
    feat_block = width // n_tp
    xf = tokens.astype(jnp.float32)
    normed_in = (
        xf * lax.rsqrt(jnp.mean(xf * xf, axis=1, keepdims=True) + eps) * in_gain.astype(jnp.float32)
    ).astype(jnp.bfloat16)
    flat_ids = expert_ids.reshape(-1)
    onehot = (flat_ids[:, None] == jnp.arange(experts, dtype=jnp.int32)[None, :]).astype(jnp.int32)
    slot = jnp.sum((jnp.cumsum(onehot, axis=0) - onehot) * onehot, axis=1)
    dest = flat_ids * capacity + slot
    token_of = jnp.arange(tok_count * top_count, dtype=jnp.int32) // top_count
    slot_token = jnp.full((experts * capacity,), tok_count, jnp.int32).at[dest].set(token_of)
    source = lax.dynamic_slice_in_dim(normed_in, lax.axis_index("tp") * feat_block, feat_block, 1)
    extended = jnp.concatenate([source, jnp.zeros((1, source.shape[1]), jnp.bfloat16)], axis=0)
    outgoing = extended[slot_token].reshape(experts, capacity, source.shape[1])
    w_gate = gate_weight[0]
    w_up = up_weight[0]
    arrived = lax.all_to_all(outgoing, "ep", split_axis=0, concat_axis=0, tiled=True).reshape(
        n_ep * capacity, feat_block
    )
    piece = lax.all_gather(arrived, "tp", axis=1, tiled=True)
    gate_pre = jnp.dot(piece, w_gate, preferred_element_type=jnp.float32)
    up_pre = jnp.dot(piece, w_up, preferred_element_type=jnp.float32)
    clamped = jnp.minimum(gate_pre, 7.0)
    bounded = jnp.clip(up_pre, -7.0, 7.0)
    act = (clamped * jax.nn.sigmoid(1.702 * clamped) * (bounded + 1.0)).astype(jnp.bfloat16)
    w_down = down_weight[0]
    summed = lax.psum_scatter(
        lax.dot_general(
            w_down, act, (((0,), (1,)), ((), ())), preferred_element_type=jnp.float32
        ).astype(jnp.bfloat16),
        "tp",
        scatter_dimension=0,
        tiled=True,
    )
    summed = summed.reshape(feat_block, n_ep, capacity)
    returned = lax.all_to_all(summed, "ep", split_axis=1, concat_axis=1, tiled=True)
    returned = returned.reshape(feat_block, experts * capacity).T
    picked = returned[dest].astype(jnp.float32).reshape(tok_count, top_count, feat_block)
    combined = jnp.sum(picked * route_weights[:, :, None], axis=1)
    squares = lax.psum(jnp.sum(combined * combined, axis=1), "tp")
    scale = lax.rsqrt(squares / width + eps)
    return (combined * scale[:, None] * out_gain.astype(jnp.float32)).astype(jnp.bfloat16)


def solution(mesh):
    placed = (
        P(("grp", "ep"), None),
        P(),
        P(("grp", "ep"), None),
        P(("grp", "ep"), None),
        P("ep", None, "tp"),
        P("ep", None, "tp"),
        P("ep", "tp", None),
        P("tp"),
    )
    return jax.shard_map(
        on_device, mesh=mesh, in_specs=placed, out_specs=P(("grp", "ep"), "tp"), check_vma=False
    )
```

time: 85 us -> 57.3 us (0.67)
  Pallas kernels: 77.6 us -> 56.4 us
  local copies, waits for them, and re-layouts: 7.15 us -> 0.71 us
    pallas_call x1, Pallas kernels: 77.6 us -> 56.4 us  [fused(): pl.pallas_call(layer_kernel, out_shape=pltpu.VMEM(piece, bf16), in_specs=...]
    unnamed x3 -> x1, local copies, waits for them, and re-layouts: 4.62 us -> 0.71 us
    reshape x2 -> x0, local copies, waits for them, and re-layouts: 2.53 us -> none  [the longest x1 1.29 us: fused(): in_gain.reshape(1, -1)]
where the time goes in v2:
time: 57.3 us; the launch traced here: 57.1 us
  Pallas kernels  56.4 us (98%)
  local copies, waits for them, and re-layouts  0.71 us (1%)
    pallas_call x1, Pallas kernels, fused(): pl.pallas_call(layer_kernel, out_shape=pltpu.VMEM(piece, bf16), in_specs=...  56.4 us

profile of v2, /device:TPU:0, one launch (start us, length us, event | category | flops | bytes accessed | tf_op | source)
XLA Modules:
  0.0 57.1 jit_solution(4526930479662862004)
XLA Ops:
  0.0 56.4 %layer.1 = bf16[256,512]{1,0:T(8,128)(2,1)S(1)} custom-call(bf16[256,2048]{1,0:T(8,128)(2,1)} %tok.1, bf16[16,128]{1,0:T(8,128)(2,1)} %bitcast.4, s32[2,256]{1,0:T(2,128)} %bitcast.5, f32[2,256]{1,0:T(2,128)} %bitcast.6, bf16[1,2048,512]{2,1,0:T(8,128)(2,1)} %wg.1, bf16[1,2048,512]{2,1,0:T(8,128)(2,1)} %wu.1, bf16[1,512,2048]{2,1,0:T(8,128)(2,1)} %wd.1, ...), custom_call_target="tpu_custom_call" | custom-call | tf_op jit(solution)/shard_map/layer/pallas_call | solution.py:298
  56.4 0.7 %copy.10 = bf16[256,512]{1,0:T(8,128)(2,1)} copy(bf16[256,512]{1,0:T(8,128)(2,1)S(1)} %layer.1) | data formatting | bytes 524288

commit v3 on v2

--- a/solution.py
+++ b/solution.py
@@ -21,28 +21,28 @@
         (2, 0), (1, 0), (2, 1), (1, 1),
     ),
     (
-        (2, 0), (1, 0), (2, 1), (1, 1),
+        (1, 0), (2, 0), (1, 1), (2, 1),
     ),
 )
 
 schedules = (
     (
-        ("C", 0, 1), ("Z", 1, 0), ("C", 0, 0), ("Z", 1, 1), ("X", 1, 0), ("Z", 3, 0),
-        ("C", 1, 0), ("X", 1, 1), ("Z", 2, 0), ("P", 1, 0), ("Q", 1, 0), ("Z", 3, 1),
-        ("C", 1, 1), ("X", 2, 0), ("P", 1, 1), ("X", 3, 0), ("Z", 2, 1), ("C", 2, 0),
-        ("X", 3, 1), ("P", 2, 0), ("Q", 1, 1), ("C", 3, 0), ("P", 3, 0), ("X", 2, 1),
-        ("C", 3, 1), ("Q", 2, 0), ("P", 3, 1), ("C", 2, 1), ("Q", 3, 0), ("P", 2, 1),
-        ("Q", 3, 1), ("P", 0, 0), ("P", 0, 1), ("Q", 2, 1), ("Q", 0, 1), ("R", 0, 1),
-        ("Q", 0, 0), ("R", 0, 0), ("O", 0, 1), ("O", 0, 0),
+        ("Z", 1, 0), ("Z", 1, 1), ("Z", 3, 0), ("C", 0, 1), ("X", 1, 0), ("X", 1, 1),
+        ("Z", 2, 0), ("C", 1, 0), ("Z", 3, 1), ("P", 1, 0), ("X", 3, 0), ("C", 1, 1),
+        ("X", 2, 0), ("Q", 1, 0), ("Z", 2, 1), ("C", 2, 0), ("X", 3, 1), ("P", 1, 1),
+        ("P", 2, 0), ("C", 3, 0), ("X", 2, 1), ("P", 3, 0), ("C", 3, 1), ("Q", 2, 0),
+        ("P", 3, 1), ("C", 2, 1), ("Q", 3, 0), ("P", 2, 1), ("C", 0, 0), ("Q", 3, 1),
+        ("P", 0, 0), ("P", 0, 1), ("Q", 2, 1), ("Q", 0, 0), ("R", 0, 0), ("Q", 1, 1),
+        ("Q", 0, 1), ("R", 0, 1), ("O", 0, 1), ("O", 0, 0),
     ),
     (
-        ("C", 0, 0), ("Z", 3, 0), ("Z", 2, 0), ("Z", 3, 1), ("C", 0, 1), ("X", 2, 0),
-        ("Z", 1, 1), ("X", 3, 0), ("Z", 2, 1), ("C", 2, 0), ("X", 3, 1), ("C", 3, 1),
-        ("Z", 1, 0), ("P", 2, 0), ("P", 0, 0), ("X", 1, 1), ("C", 3, 0), ("C", 1, 1),
-        ("P", 3, 0), ("P", 1, 1), ("Q", 1, 1), ("X", 2, 1), ("P", 3, 1), ("X", 1, 0),
-        ("C", 1, 0), ("P", 1, 0), ("C", 2, 1), ("Q", 2, 0), ("Q", 3, 0), ("P", 2, 1),
-        ("P", 0, 1), ("Q", 1, 0), ("Q", 3, 1), ("Q", 2, 1), ("Q", 0, 1), ("Q", 0, 0),
-        ("R", 0, 0), ("R", 0, 1), ("O", 0, 0), ("O", 0, 1),
+        ("Z", 3, 0), ("C", 0, 0), ("Z", 2, 0), ("Z", 1, 0), ("Z", 3, 1), ("X", 3, 0),
+        ("C", 3, 0), ("Z", 2, 1), ("X", 1, 0), ("X", 2, 0), ("C", 1, 0), ("Z", 1, 1),
+        ("P", 1, 0), ("C", 2, 0), ("X", 3, 1), ("P", 2, 0), ("C", 0, 1), ("Q", 1, 0),
+        ("X", 1, 1), ("P", 3, 0), ("C", 3, 1), ("P", 3, 1), ("X", 2, 1), ("C", 1, 1),
+        ("P", 0, 0), ("C", 2, 1), ("P", 1, 1), ("Q", 1, 1), ("Q", 2, 0), ("P", 2, 1),
+        ("Q", 3, 0), ("P", 0, 1), ("Q", 0, 0), ("Q", 3, 1), ("R", 0, 0), ("Q", 2, 1),
+        ("O", 0, 0), ("Q", 0, 1), ("R", 0, 1), ("O", 0, 1),
     ),
 )
 

time: 57.3 us -> 55.2 us (0.963)
  Pallas kernels: 56.4 us -> 53.8 us
    pallas_call x1, Pallas kernels: 56.4 us -> 53.8 us  [fused(): pl.pallas_call(layer_kernel, out_shape=pltpu.VMEM(piece, bf16), in_specs=...]
where the time goes in v3:
time: 55.2 us; the launch traced here: 54.6 us
  Pallas kernels  53.8 us (97%)
  local copies, waits for them, and re-layouts  0.71 us (1%)
    pallas_call x1, Pallas kernels, fused(): pl.pallas_call(layer_kernel, out_shape=pltpu.VMEM(piece, bf16), in_specs=...  53.8 us

profile of v3, /device:TPU:0, one launch (start us, length us, event | category | flops | bytes accessed | tf_op | source)
XLA Modules:
  0.0 54.6 jit_solution(9950424426982116421)
XLA Ops:
  0.0 53.8 %layer.1 = bf16[256,512]{1,0:T(8,128)(2,1)S(1)} custom-call(bf16[256,2048]{1,0:T(8,128)(2,1)} %tok.1, bf16[16,128]{1,0:T(8,128)(2,1)} %bitcast.4, s32[2,256]{1,0:T(2,128)} %bitcast.5, f32[2,256]{1,0:T(2,128)} %bitcast.6, bf16[1,2048,512]{2,1,0:T(8,128)(2,1)} %wg.1, bf16[1,2048,512]{2,1,0:T(8,128)(2,1)} %wu.1, bf16[1,512,2048]{2,1,0:T(8,128)(2,1)} %wd.1, ...), custom_call_target="tpu_custom_call" | custom-call | tf_op jit(solution)/shard_map/layer/pallas_call | solution.py:298
  53.8 0.7 %copy.10 = bf16[256,512]{1,0:T(8,128)(2,1)} copy(bf16[256,512]{1,0:T(8,128)(2,1)S(1)} %layer.1) | data formatting | bytes 524288

commit v4 on v3

--- a/solution.py
+++ b/solution.py
@@ -151,14 +151,15 @@
                 one(across)
             if h == 0:
                 pl.semaphore_wait(barrier, 6)
-                for i in (1, 2, 3):
-                    push(remote(table.at[i], far_table.at[z], hs.at[i], hr.at[z], ep=order[i]))
             mine, other = xbuf.at[z, p, span(h)], xbuf.at[z, across, span(h)]
             for i, k in send_order[is_middle]:
                 if k == h:
                     push(remote(mine, mine, zs.at[i, h], zr.at[z, h], ep=order[i]))
                     if i == 1 and h in whole_in:
                         push(remote(other, other, ys.at[h], yr.at[h], ep=order[1]))
+            if h == 0:
+                for i in (1, 2, 3):
+                    push(remote(table.at[i], far_table.at[z], hs.at[i], hr.at[z], ep=order[i]))
             for q in (mate, diagonal) if h in whole_in else (across, mate, diagonal):
                 one(q)
 

time: 55.2 us -> 54.1 us (0.980)
  Pallas kernels: 53.8 us -> 53 us
    pallas_call x1, Pallas kernels: 53.8 us -> 53 us  [fused(): pl.pallas_call(layer_kernel, out_shape=pltpu.VMEM(piece, bf16), in_specs=...]
where the time goes in v4:
time: 54.1 us; the launch traced here: 53.7 us
  Pallas kernels  53 us (98%)
  local copies, waits for them, and re-layouts  0.71 us (1%)
    pallas_call x1, Pallas kernels, fused(): pl.pallas_call(layer_kernel, out_shape=pltpu.VMEM(piece, bf16), in_specs=...  53 us

profile of v4, /device:TPU:0, one launch (start us, length us, event | category | flops | bytes accessed | tf_op | source)
XLA Modules:
  0.0 53.7 jit_solution(15236256631499239185)
XLA Ops:
  0.0 53.0 %layer.1 = bf16[256,512]{1,0:T(8,128)(2,1)S(1)} custom-call(bf16[256,2048]{1,0:T(8,128)(2,1)} %tok.1, bf16[16,128]{1,0:T(8,128)(2,1)} %bitcast.4, s32[2,256]{1,0:T(2,128)} %bitcast.5, f32[2,256]{1,0:T(2,128)} %bitcast.6, bf16[1,2048,512]{2,1,0:T(8,128)(2,1)} %wg.1, bf16[1,2048,512]{2,1,0:T(8,128)(2,1)} %wu.1, bf16[1,512,2048]{2,1,0:T(8,128)(2,1)} %wd.1, ...), custom_call_target="tpu_custom_call" | custom-call | tf_op jit(solution)/shard_map/layer/pallas_call | solution.py:299
  53.0 0.7 %copy.10 = bf16[256,512]{1,0:T(8,128)(2,1)} copy(bf16[256,512]{1,0:T(8,128)(2,1)S(1)} %layer.1) | data formatting | bytes 524288
